TPU v7x, 256 devices: a whole 4x4x8 slice. The times are simulated.
256 devices in a mesh: sp: 64 (over z, y, core), tp: 4 (over x).
Axes of the slice: x: 4, y: 4, z: 8, core: 2. Of those that a mesh axis runs over, the one named last changes fastest.
Arguments:
- stream: bfloat16 [8192, 2048], P('sp', 'tp'), may hold values from -40 to 40
- queries: bfloat16 [8192, 1024], P('sp', 'tp'), may hold values from -6 to 6
- keys: bfloat16 [8192, 1024], P('sp', 'tp'), may hold values from -6 to 6
- values: bfloat16 [8192, 2048], P('sp', 'tp'), may hold values from -25 to 25
- out_gate: bfloat16 [8192, 2048], P('sp', 'tp'), may hold values from -8 to 8
- input_gate: float32 [8192, 8], P('sp', 'tp'), may hold values from -9 to 350
- forget_gate: float32 [8192, 8], P('sp', 'tp'), may hold values from -4 to 20
- head_gain: float32 [2048], P('tp'), may hold values from 0.1 to 1.9
- w_out: bfloat16 [2048, 2048], P('tp'), may hold values from -0.125 to 0.125
- ffn_gain: float32 [2048], replicated, may hold values from 0.1 to 1.9
- w_gate: bfloat16 [2048, 5632], P('sp', 'tp'), may hold values from -0.125 to 0.125
- w_up: bfloat16 [2048, 5632], P('sp', 'tp'), may hold values from -0.125 to 0.125
- w_down: bfloat16 [5632, 2048], P('tp', 'sp'), may hold values from -0.078125 to 0.078125
Outputs:
- mixed: bfloat16 [8192, 2048], P('sp', 'tp')
All inputs are finite; a program needn't handle non-finite values.
Results may differ from a plain program's by a relative error of at most 0.0095.
Values may be sent and summed in bfloat16 or wider, within the bound.
A program may use at most 128 MiB of HBM per device.

v0:
```python
import jax
import jax.numpy as jnp
from jax import lax
from jax.sharding import Mesh
from jax.sharding import PartitionSpec as P

D = 2048
DQK = 128
DV = 256
BLOCK = 64
VALS = 2048
SP = ("sp_0", "sp_1", "sp_2")
precise = lax.Precision.HIGHEST
norm_eps = 1e-06
very_low = -1e30


def gather_turned(arrays, axis, dims):
    turned = [jnp.moveaxis(a, dim, 0) for a, dim in zip(arrays, dims)]
    both = jnp.concatenate([t.reshape(len(t), -1) for t in turned], axis=1)
    result, at, gathered = (lax.all_gather(both, axis, axis=0, tiled=True), 0, [])
    for t, dim in zip(turned, dims):
        slab = result[:, at : at + t[0].size].reshape(-1, *t.shape[1:])
        gathered.append(jnp.moveaxis(slab, 0, dim))
        at += t[0].size
    return tuple(gathered)


def nothing_yet(x, identity):
    return jax.tree.map(
        lambda a, e: jnp.broadcast_to(jnp.asarray(e, a.dtype), a.shape), x, identity
    )


def all_in_one(x, axis):
    leaves = jax.tree.leaves(x)
    order = sorted(range(len(leaves)), key=lambda k: -leaves[k].size)
    width = (1, *leaves[order[0]].shape)[-1]
    lines = [
        jnp.pad(leaves[k].reshape(-1), (0, -leaves[k].size % width)).reshape(-1, width)
        for k in order
    ]
    both, at, found = (lax.all_gather(jnp.concatenate(lines), axis), 0, {})
    for k, line in zip(order, lines):
        slab = both[:, at : at + len(line)].reshape(len(both), -1)
        found[k] = slab[:, : leaves[k].size].reshape(-1, *leaves[k].shape)
        at += len(line)
    numbers = iter(range(len(leaves)))
    return jax.tree.map(lambda _: found[next(numbers)], x)


def entering(x, axes, combine, identity):
    before = start = nothing_yet(x, identity)
    subtotal = x
    for axis in reversed(axes):
        peers, mine = (lax.axis_size(axis), lax.axis_index(axis))
        pieces = all_in_one(subtotal, axis)
        inside, subtotal = (start, start)
        for k in range(peers):
            passed = k < mine
            subtotal = combine(subtotal, jax.tree.map(lambda part: part[k], pieces))
            inside = jax.tree.map(lambda new, old: jnp.where(passed, new, old), subtotal, inside)
        before = combine(inside, before)
    return before


def copy_for_each(x, axis):
    peers = lax.axis_size(axis)
    return lax.all_to_all(jnp.broadcast_to(x[None], (peers, *x.shape)), axis, 0, 0, tiled=True)


def over_copies(x, axis):
    everything = copy_for_each(x, axis)
    return jnp.sum(everything, axis=0)


def cut_along(x, dim, peers):
    shape = x.shape
    parts = x.reshape(*shape[:dim], peers, shape[dim] // peers, *shape[dim + 1 :])
    return jnp.moveaxis(parts, dim, 0)


def summed_on_arrival(x, axis, dim):
    parts = cut_along(x, dim, lax.axis_size(axis))
    arrived = lax.all_to_all(parts, axis, split_axis=0, concat_axis=0, tiled=True)
    return arrived.astype(jnp.float32).sum(axis=0)


def in_order(parts, dim):
    shape = list(parts.shape[1:])
    shape[dim] *= parts.shape[0]
    return jnp.moveaxis(parts, 0, dim).reshape(shape)


def gathered_copies(x, axis, dim):
    parts = copy_for_each(x, axis)
    return in_order(parts, dim)


def block_summary(key_blk, value_blk, input_blk, decay_sum):
    decay_total = decay_sum[..., -1]
    log_weight = decay_total[..., None] - decay_sum + input_blk
    weight_peak = jnp.max(log_weight, axis=-1)
    weights = jnp.exp(log_weight - weight_peak[..., None])
    state_mat = jnp.einsum(
        "...ld,...le->...de", weights[..., None] * key_blk, value_blk, precision=precise
    )
    state_vec = jnp.einsum("...l,...ld->...d", weights, key_blk, precision=precise)
    return (state_mat, state_vec, weight_peak, decay_total)


def combine(earlier, later):
    ceiling = jnp.maximum(later[3] + earlier[2], later[2])
    former = jnp.exp(later[3] + earlier[2] - ceiling)
    latter = jnp.exp(later[2] - ceiling)
    return (
        former[..., None, None] * earlier[0] + latter[..., None, None] * later[0],
        former[..., None] * earlier[1] + latter[..., None] * later[1],
        ceiling,
        earlier[3] + later[3],
    )


def block_output(
    query_blk, key_blk, value_blk, input_blk, decay_sum, state_mat, state_vec, state_peak
):
    block_len = query_blk.shape[-2]
    causal = jnp.tril(jnp.ones((block_len, block_len), jnp.bool_))
    log_pair = jnp.where(
        causal,
        decay_sum[..., :, None] - decay_sum[..., None, :] + input_blk[..., None, :],
        -jnp.inf,
    )
    log_carry = decay_sum + state_peak[..., None]
    row_peak = jnp.maximum(log_carry, jnp.max(log_pair, axis=-1))
    scores = jnp.einsum("...ld,...sd->...ls", query_blk, key_blk, precision=precise) * jnp.exp(
        log_pair - row_peak[..., None]
    )
    carried = jnp.exp(log_carry - row_peak)
    numer = jnp.einsum("...ls,...se->...le", scores, value_blk, precision=precise) + carried[
        ..., None
    ] * jnp.einsum("...ld,...de->...le", query_blk, state_mat, precision=precise)
    normer = jnp.sum(scores, axis=-1) + carried * jnp.einsum(
        "...ld,...d->...l", query_blk, state_vec, precision=precise
    )
    denom = jnp.maximum(jnp.abs(normer), jnp.exp(-row_peak))
    return numer / denom[..., None]


def local(
    stream,
    queries,
    keys,
    values,
    out_gate,
    input_gate,
    forget_gate,
    head_gain,
    w_out,
    ffn_gain,
    w_gate,
    w_up,
    w_down,
):
    gate_full, up_full, down_full = gather_turned((w_gate, w_up, w_down), SP, (0, 0, 1))
    count_of_rows = stream.shape[0]
    head_count = input_gate.shape[1]
    blocks = count_of_rows // BLOCK

    def to_blocks(array, col_width):
        return (
            array.astype(jnp.float32)
            .reshape(blocks, BLOCK, head_count, col_width)
            .transpose(2, 0, 1, 3)
        )

    query_blk = to_blocks(queries, DQK) * DQK ** (-0.5)
    key_blk = to_blocks(keys, DQK)
    value_blk = to_blocks(values, DV)
    input_blk = input_gate.reshape(blocks, BLOCK, head_count).transpose(2, 0, 1)
    decay_sum = jnp.cumsum(
        jax.nn.log_sigmoid(forget_gate).reshape(blocks, BLOCK, head_count).transpose(2, 0, 1),
        axis=-1,
    )
    summary = block_summary(key_blk, value_blk, input_blk, decay_sum)
    identity = (
        jnp.zeros((head_count, DQK, DV), jnp.float32),
        jnp.zeros((head_count, DQK), jnp.float32),
        jnp.full((head_count,), very_low, jnp.float32),
        jnp.zeros((head_count,), jnp.float32),
    )

    def advance(carry, piece):
        return (combine(carry, piece), carry)

    local_total, prefix = lax.scan(
        advance, identity, jax.tree.map(lambda array: jnp.moveaxis(array, 1, 0), summary)
    )
    carry_in = entering(local_total, SP, combine, identity)
    start = combine(
        jax.tree.map(lambda array: array[:, None], carry_in),
        jax.tree.map(lambda array: jnp.moveaxis(array, 0, 1), prefix),
    )
    mixed_heads = block_output(
        query_blk, key_blk, value_blk, input_blk, decay_sum, start[0], start[1], start[2]
    )
    head_rows = mixed_heads.transpose(1, 2, 0, 3).reshape(count_of_rows, head_count, DV)
    local_sq = jnp.sum(head_rows * head_rows, axis=(1, 2))
    total_sq = over_copies(local_sq, "tp")
    row_scale = lax.rsqrt(total_sq / VALS + norm_eps)
    gated = (
        head_rows
        * row_scale[:, None, None]
        * head_gain.reshape(head_count, DV)
        * jax.nn.sigmoid(out_gate.astype(jnp.float32).reshape(count_of_rows, head_count, DV))
    )
    heads_out = gated.reshape(count_of_rows, head_count * DV).astype(jnp.bfloat16)
    partial_value = jnp.dot(heads_out, w_out, preferred_element_type=jnp.float32)
    col_width = stream.shape[1]
    col_start = lax.axis_index("tp") * col_width
    mixer_own = summed_on_arrival(partial_value.astype(jnp.bfloat16), "tp", 1)
    resid_own = (stream.astype(jnp.float32) + mixer_own).astype(jnp.bfloat16)
    resid_f = resid_own.astype(jnp.float32)
    square_total = over_copies(jnp.sum(resid_f * resid_f, axis=-1), "tp")
    gain_own = lax.dynamic_slice_in_dim(ffn_gain, col_start, col_width)
    normed_own = (resid_f * lax.rsqrt(square_total / D + norm_eps)[:, None] * gain_own).astype(
        jnp.bfloat16
    )
    normed = gathered_copies(normed_own, "tp", 1)
    gate_act = jnp.dot(normed, gate_full, preferred_element_type=jnp.float32)
    up_act = jnp.dot(normed, up_full, preferred_element_type=jnp.float32)
    hidden = (jax.nn.silu(gate_act) * up_act).astype(jnp.bfloat16)
    term = jnp.dot(hidden, down_full, preferred_element_type=jnp.float32)
    down_own = summed_on_arrival(term.astype(jnp.bfloat16), "tp", 1)
    return (resid_own.astype(jnp.float32) + down_own).astype(jnp.bfloat16)


def solution(mesh):
    split = Mesh(mesh.devices.reshape(8, 4, 2, mesh.shape["tp"]), ("sp_0", "sp_1", "sp_2", "tp"))
    in_specs = (
        P(SP, "tp"),
        P(SP, "tp"),
        P(SP, "tp"),
        P(SP, "tp"),
        P(SP, "tp"),
        P(SP, "tp"),
        P(SP, "tp"),
        P("tp"),
        P("tp", None),
        P(),
        P(SP, "tp"),
        P(SP, "tp"),
        P("tp", SP),
    )
    out_specs = P(SP, "tp")
    return jax.shard_map(local, mesh=split, in_specs=in_specs, out_specs=out_specs, check_vma=False)
```

profile of v0, /device:TPU:1, one launch (start us, length us, event | category | flops | bytes accessed | tf_op | source)
XLA Modules:
  0.0 230.6 jit_solution(16289289867176333970)
XLA Ops:
  11.8 2.1 while.25
  14.5 5.0 %all-gather.3 = f32[2,259,256]{2,1,0:T(8,128)S(1)} all-gather(f32[1,259,256]{2,1,0:T(8,128)S(1)} %maximum_bitcast_fusion), channel_id=2, replica_groups=mesh['sp_0'=8,'sp_1'=4,'sp_2'=2,'tp'=4] {'sp_2'}, dimensions={0}, use_global_device_ids=true | all-gather | bytes 795648 | tf_op jit(solution)/shard_map/all_gather | solution.py:43
  21.5 25.7 %all-gather.12.cloned.1.call-done = f32[4,259,256]{2,1,0:T(8,128)} async-done(((f32[1,259,256]{2,1,0:T(8,128)}), f32[4,259,256]{2,1,0:T(8,128)}) %all-gather.12.cloned.1.call-update) | async-done | bytes 1060880 | tf_op jit(solution)/shard_map/all_gather | solution.py:43
  48.9 1.5 fusion.43
  55.7 1.4 fusion.153
  57.0 2.0 fusion.154
  59.0 33.0 %all-gather.14.cloned.1.call-done = f32[8,259,256]{2,1,0:T(8,128)} async-done(((f32[1,259,256]{2,1,0:T(8,128)}), f32[8,259,256]{2,1,0:T(8,128)}) %all-gather.14.cloned.1.call-update) | async-done | bytes 2121744 | tf_op jit(solution)/shard_map/all_gather | solution.py:43
  94.5 1.2 subtract_exponential_fusion.23
  96.3 1.3 fusion.85
  97.5 1.3 copy.70
  98.8 1.3 add_maximum_fusion.1
  100.1 1.3 copy.72
  109.0 1.2 fusion.159
  111.5 1.6 fusion.151
  115.6 3.7 %all-to-all-start = ((f32[4,1,128]{2,1,0:T(1,128)}), f32[4,1,128]{2,1,0:T(1,128)S(1)}, u32[]{:S(2)}, u32[]{:S(2)}) async-start(f32[4,1,128]{2,1,0:T(1,128)} %broadcast_in_dim.49), calls=%async_computation | async-start | bytes 4096 | tf_op jit(solution)/shard_map/all_to_all | solution.py:69
  119.5 3.8 %all-to-all-done = f32[4,1,128]{2,1,0:T(1,128)S(1)} async-done(((f32[4,1,128]{2,1,0:T(1,128)}), f32[4,1,128]{2,1,0:T(1,128)S(1)}, u32[]{:S(2)}, u32[]{:S(2)}) %all-to-all-start) | async-done | bytes 2080 | tf_op jit(solution)/shard_map/all_to_all | solution.py:69
  124.0 9.3 %all_to_all.27 = bf16[4,128,512]{2,1,0:T(8,128)(2,1)S(1)} all-to-all(bf16[4,128,512]{2,1,0:T(8,128)(2,1)S(1)} %bitcast.624), channel_id=1, replica_groups=mesh['sp_0'=8,'sp_1'=4,'sp_2'=2,'tp'=4] {'tp'}, dimensions={0} | all-to-all | bytes 1048576 | tf_op jit(solution)/shard_map/all_to_all | solution.py:85
  134.1 3.2 %all-to-all-start.2 = ((f32[4,1,128]{2,1,0:T(1,128)}), f32[4,1,128]{2,1,0:T(1,128)S(1)}, u32[]{:S(2)}, u32[]{:S(2)}) async-start(f32[4,1,128]{2,1,0:T(1,128)} %broadcast_in_dim.50), calls=%async_computation.2 | async-start | bytes 4096 | tf_op jit(solution)/shard_map/all_to_all | solution.py:69
  138.1 3.3 %all-to-all-done.2 = f32[4,1,128]{2,1,0:T(1,128)S(1)} async-done(((f32[4,1,128]{2,1,0:T(1,128)}), f32[4,1,128]{2,1,0:T(1,128)S(1)}, u32[]{:S(2)}, u32[]{:S(2)}) %all-to-all-start.2) | async-done | bytes 2080 | tf_op jit(solution)/shard_map/all_to_all | solution.py:69
  141.7 9.3 %all_to_all.28 = bf16[4,128,512]{1,2,0:T(8,128)(2,1)S(1)} all-to-all(bf16[4,128,512]{1,2,0:T(8,128)(2,1)S(1)} %broadcast_in_dim.51), channel_id=1, replica_groups=mesh['sp_0'=8,'sp_1'=4,'sp_2'=2,'tp'=4] {'tp'}, dimensions={0} | all-to-all | bytes 1048576 | tf_op jit(solution)/shard_map/all_to_all | solution.py:69
  151.0 47.5 %all-gather.10.cloned.1.call-done = bf16[2048,4224]{1,0:T(8,128)(2,1)} async-done(((bf16[32,4224]{1,0:T(8,128)(2,1)}), bf16[2048,4224]{1,0:T(8,128)(2,1)}) %all-gather.10.cloned.1.call-update) | async-done | bytes 17301520 | tf_op jit(solution)/shard_map/all_gather | solution.py:21
  198.5 4.5 %fusion.15 = f32[128,1408]{1,0:T(8,128)} fusion(bf16[128,2048]{0,1:T(8,128)(2,1)S(1)} %bitcast.641, bf16[2048,4224]{1,0:T(8,128)(2,1)} %all-gather.10.cloned.1.call-done), kind=kOutput, calls=%fused_computation.26 | convolution fusion | flops 738197504 | bytes 7012352 | tf_op jit(solution)/shard_map/dot_general | solution.py:230
  203.0 7.4 %fusion.20 = bf16[128,2048]{1,0:T(8,128)(2,1)S(1)} fusion(bf16[2048,4224]{1,0:T(8,128)(2,1)} %all-gather.10.cloned.1.call-done, bf16[128,2048]{0,1:T(8,128)(2,1)S(1)} %bitcast.642, f32[128,1408]{1,0:T(8,128)} %fusion.15), kind=kOutput, calls=%fused_computation.29 | convolution fusion | flops 1477738496 | bytes 13303808 | tf_op jit(solution)/shard_map/dot_general | solution.py:233
  210.5 12.8 %all_to_all.29 = bf16[4,128,512]{2,1,0:T(8,128)(2,1)S(1)} all-to-all(bf16[4,128,512]{2,1,0:T(8,128)(2,1)S(1)} %bitcast.625), channel_id=1, replica_groups=mesh['sp_0'=8,'sp_1'=4,'sp_2'=2,'tp'=4] {'tp'}, dimensions={0} | all-to-all | bytes 1048576 | tf_op jit(solution)/shard_map/all_to_all | solution.py:85
  (272 shorter events, 33.5 us)
Async XLA Ops:
  6.5 116.8 %copy-start = (bf16[512,2048]{1,0:T(8,128)(2,1)S(1)}, bf16[512,2048]{1,0:T(8,128)(2,1)}, u32[]{:S(2)}) copy-start(bf16[512,2048]{1,0:T(8,128)(2,1)} %param.23) | copy-start | bytes 6291460
  6.5 40.7 %all-gather.12.cloned.1.call-start = ((), (), s32[]{:S(2)}) async-start(), calls=%async_computation.6 | async-start | bytes 1351680 | tf_op jit(solution)/shard_map/all_gather | solution.py:43
  8.0 46.2 %copy-start.5 = (f32[2,2,64]{2,1,0:T(2,128)}, f32[2,2,64]{2,1,0:T(2,128)S(1)}, u32[]{:S(2)}) copy-start(f32[2,2,64]{2,1,0:T(2,128)S(1)} %reduce_window_sum.13) | copy-start | bytes 3076
  8.9 45.3 %copy-start.13 = (f32[2,64,2]{1,0,2:T(2,128)}, f32[2,64,2]{1,0,2:T(2,128)S(1)}, u32[]{:S(2)}) copy-start(f32[2,64,2]{1,0,2:T(2,128)S(1)} %reshape.3324) | copy-start | bytes 3076
  19.5 33.0 %copy-start.7 = (bf16[1408,32]{0,1:T(8,128)(2,1)S(1)}, bf16[1408,32]{0,1:T(8,128)(2,1)}, u32[]{:S(2)}) copy-start(bf16[1408,32]{0,1:T(8,128)(2,1)} %param.27) | copy-start | bytes 270340
  19.5 33.1 %copy-start.8 = (bf16[32,1408]{1,0:T(8,128)(2,1)S(1)}, bf16[32,1408]{1,0:T(8,128)(2,1)}, u32[]{:S(2)}) copy-start(bf16[32,1408]{1,0:T(8,128)(2,1)} %param.26) | copy-start | bytes 270340
  19.5 33.1 %copy-start.9 = (bf16[32,1408]{1,0:T(8,128)(2,1)S(1)}, bf16[32,1408]{1,0:T(8,128)(2,1)}, u32[]{:S(2)}) copy-start(bf16[32,1408]{1,0:T(8,128)(2,1)} %param.25) | copy-start | bytes 270340
  19.7 28.4 %copy-start.50 = (f32[2]{0:T(128)}, f32[2]{0:T(128)S(1)}, u32[]{:S(2)}) copy-start(f32[2]{0:T(128)S(1)} %get-tuple-element.309) | copy-start | bytes 28
  20.4 33.1 %copy-start.10 = (bf16[128,256]{1,0:T(8,128)(2,1)S(1)}, bf16[128,256]{1,0:T(8,128)(2,1)}, u32[]{:S(2)}) copy-start(bf16[128,256]{1,0:T(8,128)(2,1)} %param.16) | copy-start | bytes 196612
  21.5 70.5 %all-gather.14.cloned.1.call-start = ((), (), s32[]{:S(2)}) async-start(), calls=%async_computation.7 | async-start | bytes 2433024 | tf_op jit(solution)/shard_map/all_gather | solution.py:43
  48.1 6.8 %copy-start.15 = (f32[4,1,256]{2,0,1:T(4,128)}, f32[4,1,256]{2,0,1:T(4,128)S(1)}, u32[]{:S(2)}) copy-start(f32[4,1,256]{2,0,1:T(4,128)S(1)} %copy.153) | copy-start | bytes 12292
  48.1 6.8 %copy-start.27 = (f32[2]{0:T(128)}, f32[2]{0:T(128)S(1)}, u32[]{:S(2)}) copy-start(f32[2]{0:T(128)S(1)} %get-tuple-element.241) | copy-start | bytes 28
  48.2 6.8 %copy-start.23 = (f32[2]{0:T(128)}, f32[2]{0:T(128)S(1)}, u32[]{:S(2)}) copy-start(f32[2]{0:T(128)S(1)} %get-tuple-element.243) | copy-start | bytes 28
  48.2 6.8 %copy-start.34 = (f32[2]{0:T(128)}, f32[2]{0:T(128)S(1)}, u32[]{:S(2)}) copy-start(f32[2]{0:T(128)S(1)} %get-tuple-element.242) | copy-start | bytes 28
  48.2 6.8 %copy-start.36 = (f32[2]{0:T(128)}, f32[2]{0:T(128)S(1)}, u32[]{:S(2)}) copy-start(f32[2]{0:T(128)S(1)} %get-tuple-element.305) | copy-start | bytes 28
  48.2 6.7 %copy-start.28 = (f32[2]{0:T(128)}, f32[2]{0:T(128)S(1)}, u32[]{:S(2)}) copy-start(f32[2]{0:T(128)S(1)} %get-tuple-element.245) | copy-start | bytes 28
  52.5 146.0 %all-gather.10.cloned.1.call-start = ((), (), s32[]{:S(2)}) async-start(), calls=%async_computation.5 | async-start | bytes 17571840 | tf_op jit(solution)/shard_map/all_gather | solution.py:21
  55.6 47.2 %copy-start.6 = (f32[2,2,64]{2,1,0:T(2,128)S(1)}, f32[2,2,64]{2,1,0:T(2,128)}, u32[]{:S(2)}) copy-start(f32[2,2,64]{2,1,0:T(2,128)} %copy-done.5) | copy-start | bytes 3076
  55.7 53.3 %copy-start.14 = (f32[2,64,2]{1,0,2:T(2,128)S(1)}, f32[2,64,2]{1,0,2:T(2,128)}, u32[]{:S(2)}) copy-start(f32[2,64,2]{1,0,2:T(2,128)} %copy-done.13) | copy-start | bytes 3076
  114.2 9.2 %copy-start.64 = (bf16[128,512]{1,0:T(8,128)(2,1)S(1)}, bf16[128,512]{1,0:T(8,128)(2,1)}, u32[]{:S(2)}) copy-start(bf16[128,512]{1,0:T(8,128)(2,1)} %param.19) | copy-start | bytes 393220
  114.2 9.2 %copy-start.65 = (f32[512]{0:T(512)S(1)}, f32[512]{0:T(512)}, u32[]{:S(2)}) copy-start(f32[512]{0:T(512)} %param.22) | copy-start | bytes 6148
  115.6 7.7 %all-to-all-start = ((f32[4,1,128]{2,1,0:T(1,128)}), f32[4,1,128]{2,1,0:T(1,128)S(1)}, u32[]{:S(2)}, u32[]{:S(2)}) async-start(f32[4,1,128]{2,1,0:T(1,128)} %broadcast_in_dim.49), calls=%async_computation | async-start | bytes 4096 | tf_op jit(solution)/shard_map/all_to_all | solution.py:69
  123.9 9.5 %copy-start.4 = (bf16[128,512]{1,0:T(8,128)(2,1)S(1)}, bf16[128,512]{1,0:T(8,128)(2,1)}, u32[]{:S(2)}) copy-start(bf16[128,512]{1,0:T(8,128)(2,1)} %param.15) | copy-start | bytes 393220
  134.1 7.3 %all-to-all-start.2 = ((f32[4,1,128]{2,1,0:T(1,128)}), f32[4,1,128]{2,1,0:T(1,128)S(1)}, u32[]{:S(2)}, u32[]{:S(2)}) async-start(f32[4,1,128]{2,1,0:T(1,128)} %broadcast_in_dim.50), calls=%async_computation.2 | async-start | bytes 4096 | tf_op jit(solution)/shard_map/all_to_all | solution.py:69
  (47 other events, 104.6 us)
Sparse Core Ops, SparseCore 0:
  21.6 25.6 all-gather.11
  52.7 39.3 all-gather.13
  94.7 103.7 all-gather.9
where the time goes:
time: 232 us; the launch traced here: 231 us
  waiting for transfers between devices  113 us (49%)
  blocking collectives  36.5 us (16%)
  other arithmetic  22.5 us (10%)
  local copies, waits for them, and re-layouts  20.5 us (9%)
  matrix products  16.5 us (7%)
  between operations  14.3 us (6%)
  starting transfers between devices  6.98 us (3%)
    all_gather x2, waiting for transfers between devices, all_in_one(): both, at, found = (lax.all_gather(jnp.concatenate(lines), axis), 0, {})  58.7 us
    all_gather x1, waiting for transfers between devices, gather_turned(): lax.all_gather(both, axis, axis=0, tiled=True)  47.5 us
    all_to_all x2, blocking collectives, summed_on_arrival(): lax.all_to_all(parts, axis, split_axis=0, concat_axis=0, tiled=True)  22.1 us
    all_to_all x1, blocking collectives, copy_for_each(): lax.all_to_all(jnp.broadcast_to(x[None], (peers, *x.shape)), axis, 0, 0,...  9.34 us
    dot_general x1, matrix products, local(): term = jnp.dot(hidden, down_full, preferred_element_type=jnp.float32)  7.41 us
    all_to_all x2, waiting for transfers between devices, copy_for_each(): lax.all_to_all(jnp.broadcast_to(x[None], (peers, *x.shape)), axis, 0, 0,...  7.08 us
    all_to_all x2, starting transfers between devices, copy_for_each(): lax.all_to_all(jnp.broadcast_to(x[None], (peers, *x.shape)), axis, 0, 0,...  6.89 us
    slice x6, local copies, waits for them, and re-layouts, entering(): subtotal = combine(subtotal, jax.tree.map(lambda part: part[k], pieces))  6.41 us
  transfers between devices with their start and end apart: 5, of which 5 were waited for; matrix products, arithmetic and copies ran while one was open for 14% of the time, Pallas kernels for 0%

commit v1 on v0

--- a/solution.py
+++ b/solution.py
@@ -15,10 +15,22 @@
 very_low = -1e30
 
 
+def arrange_groups_all(which_axis, raw):
+    return jnp.concatenate(
+        lax.all_to_all(
+            jnp.stack([raw] * lax.psum(1, which_axis), axis=0),
+            axis_name=which_axis,
+            split_axis=0,
+            concat_axis=0,
+        ),
+        0,
+    )
+
+
 def gather_turned(arrays, axis, dims):
     turned = [jnp.moveaxis(a, dim, 0) for a, dim in zip(arrays, dims)]
     both = jnp.concatenate([t.reshape(len(t), -1) for t in turned], axis=1)
-    result, at, gathered = (lax.all_gather(both, axis, axis=0, tiled=True), 0, [])
+    result, at, gathered = (arrange_groups_all(axis, both), 0, [])
     for t, dim in zip(turned, dims):
         slab = result[:, at : at + t[0].size].reshape(-1, *t.shape[1:])
         gathered.append(jnp.moveaxis(slab, 0, dim))

time: 232 us -> 584 us (2.52)
  blocking collectives: 36.5 us -> 421 us
  waiting for transfers between devices: 113 us -> 73.5 us
  local copies, waits for them, and re-layouts: 20.5 us -> 27.2 us
    all_to_all x1, blocking collectives: 9.34 us -> 395 us  [arrange_groups_all(): lax.all_to_all(jnp.stack([raw] * lax.psum(1, which_axis), axis=0), axis_n...]
    all_gather x1 -> x0, waiting for transfers between devices: 47.5 us -> none  [gather_turned(): lax.all_gather(both, axis, axis=0, tiled=True)]
    all_to_all x2 -> x3, waiting for transfers between devices: 7.08 us -> 13.9 us  [copy_for_each(): lax.all_to_all(jnp.broadcast_to(x[None], (peers, *x.shape)), axis, 0, 0,...]
  transfers between devices with their start and end apart: 5 -> 5, of which waited for: 5 -> 5; matrix products, arithmetic and copies ran while one was open for 14% -> 1% of each run, Pallas kernels for 0% -> 0%
where the time goes in v1:
time: 584 us; the launch traced here: 583 us
  blocking collectives  421 us (72%)
  waiting for transfers between devices  73.5 us (13%)
  local copies, waits for them, and re-layouts  27.2 us (5%)
  other arithmetic  22.4 us (4%)
  matrix products  14.8 us (3%)
  between operations  14.4 us (2%)
  starting transfers between devices  10.4 us (2%)
    all_to_all x1, blocking collectives, arrange_groups_all(): lax.all_to_all(jnp.stack([raw] * lax.psum(1, which_axis), axis=0), axis_n...  395 us
    all_gather x2, waiting for transfers between devices, all_in_one(): both, at, found = (lax.all_gather(jnp.concatenate(lines), axis), 0, {})  59.5 us
    all_to_all x2, blocking collectives, summed_on_arrival(): lax.all_to_all(parts, axis, split_axis=0, concat_axis=0, tiled=True)  21 us
    all_to_all x3, waiting for transfers between devices, copy_for_each(): lax.all_to_all(jnp.broadcast_to(x[None], (peers, *x.shape)), axis, 0, 0,...  13.9 us
  transfers between devices with their start and end apart: 5, of which 5 were waited for; matrix products, arithmetic and copies ran while one was open for 1% of the time, Pallas kernels for 0%

profile of v1, /device:TPU:1, one launch (start us, length us, event | category | flops | bytes accessed | tf_op | source)
XLA Modules:
  0.0 583.2 jit_solution(15405251119930633748)
XLA Ops:
  11.8 2.1 while.25
  14.0 5.0 all-gather.3
  20.8 25.7 %all-gather.9.cloned.1.call-done = f32[4,259,256]{2,1,0:T(8,128)} async-done(((f32[1,259,256]{2,1,0:T(8,128)}), f32[4,259,256]{2,1,0:T(8,128)}) %all-gather.9.cloned.1.call-update) | async-done | bytes 1060880 | tf_op jit(solution)/shard_map/all_gather | solution.py:55
  49.5 1.5 fusion.43
  54.1 1.3 fusion.153
  55.5 2.0 fusion.154
  57.5 33.8 %all-gather.11.cloned.1.call-done = f32[8,259,256]{2,1,0:T(8,128)} async-done(((f32[1,259,256]{2,1,0:T(8,128)}), f32[8,259,256]{2,1,0:T(8,128)}) %all-gather.11.cloned.1.call-update) | async-done | bytes 2121744 | tf_op jit(solution)/shard_map/all_gather | solution.py:55
  99.3 1.3 copy.70
  100.6 1.3 copy.72
  109.6 1.6 fusion.151
  111.3 1.9 multiply_add_fusion
  114.6 3.7 all-to-all-start
  118.5 3.8 all-to-all-done
  122.4 1.4 convolution_convert_fusion
  123.9 9.3 %all_to_all.32 = bf16[4,128,512]{2,1,0:T(8,128)(2,1)S(1)} all-to-all(bf16[4,128,512]{2,1,0:T(8,128)(2,1)S(1)} %bitcast.627), channel_id=1, replica_groups=mesh['sp_0'=8,'sp_1'=4,'sp_2'=2,'tp'=4] {'tp'}, dimensions={0} | all-to-all | bytes 1048576 | tf_op jit(solution)/shard_map/all_to_all | solution.py:97
  134.0 3.2 all-to-all-start.2
  138.0 3.3 all-to-all-done.2
  142.4 3.5 all-to-all-start.3
  145.9 6.8 %all-to-all-done.3 = bf16[4,128,512]{1,2,0:T(8,128)(2,1)S(1)} async-done(((bf16[4,128,512]{1,2,0:T(8,128)(2,1)}), bf16[4,128,512]{1,2,0:T(8,128)(2,1)S(1)}, u32[]{:S(2)}, u32[]{:S(2)}) %all-to-all-start.3) | async-done | bytes 524320 | tf_op jit(solution)/shard_map/all_to_all | solution.py:81
  154.1 394.5 %all_to_all.33 = bf16[64,32,4224]{2,1,0:T(8,128)(2,1)S(1)} all-to-all(bf16[64,32,4224]{2,1,0:T(8,128)(2,1)S(1)} %stack.2), channel_id=1, replica_groups=mesh['sp_0'=8,'sp_1'=4,'sp_2'=2,'tp'=4] {'sp_0','sp_1','sp_2'}, dimensions={0} | all-to-all | bytes 34603008 | tf_op jit(solution)/shard_map/all_to_all | solution.py:20
  548.6 6.0 %copy-done.1 = bf16[64,32,4224]{2,1,0:T(8,128)(2,1)} copy-done((bf16[64,32,4224]{2,1,0:T(8,128)(2,1)}, bf16[64,32,4224]{2,1,0:T(8,128)(2,1)S(1)}, u32[]{:S(2)}) %copy-start.1) | copy-done | bytes 17301528
  554.6 1.9 fusion.15
  556.5 7.4 %fusion.20 = bf16[128,2048]{1,0:T(8,128)(2,1)S(1)} fusion(bf16[2048,4224]{1,0:T(8,128)(2,1)} %bitcast.626, bf16[128,2048]{0,1:T(8,128)(2,1)S(1)} %bitcast.645, f32[128,1408]{1,0:T(8,128)} %fusion.15), kind=kOutput, calls=%fused_computation.29 | convolution fusion | flops 1477738496 | bytes 13303808 | tf_op jit(solution)/shard_map/dot_general | solution.py:245
  563.9 11.7 %all_to_all.34 = bf16[4,128,512]{2,1,0:T(8,128)(2,1)S(1)} all-to-all(bf16[4,128,512]{2,1,0:T(8,128)(2,1)S(1)} %bitcast.628), channel_id=1, replica_groups=mesh['sp_0'=8,'sp_1'=4,'sp_2'=2,'tp'=4] {'tp'}, dimensions={0} | all-to-all | bytes 1048576 | tf_op jit(solution)/shard_map/all_to_all | solution.py:97
  (228 shorter events, 36.6 us)
Async XLA Ops:
  6.5 115.9 %copy-start = (bf16[512,2048]{1,0:T(8,128)(2,1)S(1)}, bf16[512,2048]{1,0:T(8,128)(2,1)}, u32[]{:S(2)}) copy-start(bf16[512,2048]{1,0:T(8,128)(2,1)} %param.23) | copy-start | bytes 6291460
  6.5 39.9 %all-gather.9.cloned.1.call-start = ((), (), s32[]{:S(2)}) async-start(), calls=%async_computation.6 | async-start | bytes 1351680 | tf_op jit(solution)/shard_map/all_gather | solution.py:55
  8.3 44.4 %copy-start.11 = (f32[2,64,2]{1,0,2:T(2,128)}, f32[2,64,2]{1,0,2:T(2,128)S(1)}, u32[]{:S(2)}) copy-start(f32[2,64,2]{1,0,2:T(2,128)S(1)} %reshape.3329) | copy-start | bytes 3076
  8.7 43.9 %copy-start.5 = (f32[2,2,64]{2,1,0:T(2,128)}, f32[2,2,64]{2,1,0:T(2,128)S(1)}, u32[]{:S(2)}) copy-start(f32[2,2,64]{2,1,0:T(2,128)S(1)} %reduce_window_sum.13) | copy-start | bytes 3076
  11.1 39.9 %copy-start.3 = (bf16[2,64,2,128]{3,2,1,0:T(2,128)(2,1)}, bf16[2,64,2,128]{3,2,1,0:T(2,128)(2,1)S(1)}, u32[]{:S(2)}) copy-start(bf16[2,64,2,128]{3,2,1,0:T(2,128)(2,1)S(1)} %reshape.3327) | copy-start | bytes 196612
  11.8 40.1 %copy-start.9 = (bf16[128,256]{1,0:T(8,128)(2,1)S(1)}, bf16[128,256]{1,0:T(8,128)(2,1)}, u32[]{:S(2)}) copy-start(bf16[128,256]{1,0:T(8,128)(2,1)} %param.16) | copy-start | bytes 196612
  13.9 39.5 %copy-start.13 = (f32[2,2]{1,0:T(2,128)}, f32[2,2]{1,0:T(2,128)S(1)}, u32[]{:S(2)}) copy-start(f32[2,2]{1,0:T(2,128)S(1)} %get-tuple-element.84) | copy-start | bytes 52
  13.9 39.5 %copy-start.38 = (f32[2,2]{1,0:T(2,128)}, f32[2,2]{1,0:T(2,128)S(1)}, u32[]{:S(2)}) copy-start(f32[2,2]{1,0:T(2,128)S(1)} %get-tuple-element.79) | copy-start | bytes 52
  13.9 39.5 %copy-start.39 = (f32[2,2,128]{2,1,0:T(2,128)}, f32[2,2,128]{2,1,0:T(2,128)S(1)}, u32[]{:S(2)}) copy-start(f32[2,2,128]{2,1,0:T(2,128)S(1)} %get-tuple-element.86) | copy-start | bytes 6148
  19.0 28.4 %copy-start.29 = (f32[2]{0:T(128)}, f32[2]{0:T(128)S(1)}, u32[]{:S(2)}) copy-start(f32[2]{0:T(128)S(1)} %get-tuple-element.248) | copy-start | bytes 28
  19.1 28.2 %copy-start.21 = (f32[2]{0:T(128)}, f32[2]{0:T(128)S(1)}, u32[]{:S(2)}) copy-start(f32[2]{0:T(128)S(1)} %get-tuple-element.251) | copy-start | bytes 28
  19.1 28.3 %copy-start.22 = (f32[2]{0:T(128)}, f32[2]{0:T(128)S(1)}, u32[]{:S(2)}) copy-start(f32[2]{0:T(128)S(1)} %get-tuple-element.310) | copy-start | bytes 28
  19.1 28.3 %copy-start.32 = (f32[2]{0:T(128)}, f32[2]{0:T(128)S(1)}, u32[]{:S(2)}) copy-start(f32[2]{0:T(128)S(1)} %get-tuple-element.309) | copy-start | bytes 28
  19.1 28.4 %copy-start.31 = (f32[2]{0:T(128)}, f32[2]{0:T(128)S(1)}, u32[]{:S(2)}) copy-start(f32[2]{0:T(128)S(1)} %get-tuple-element.250) | copy-start | bytes 28
  19.1 28.3 %copy-start.40 = (f32[2]{0:T(128)}, f32[2]{0:T(128)S(1)}, u32[]{:S(2)}) copy-start(f32[2]{0:T(128)S(1)} %subtract_exponential_fusion.31) | copy-start | bytes 28
  20.7 70.6 %all-gather.11.cloned.1.call-start = ((), (), s32[]{:S(2)}) async-start(), calls=%async_computation.7 | async-start | bytes 2433024 | tf_op jit(solution)/shard_map/all_gather | solution.py:55
  108.8 13.6 %copy-start.43 = (f32[512]{0:T(512)S(1)}, f32[512]{0:T(512)}, u32[]{:S(2)}) copy-start(f32[512]{0:T(512)} %param.22) | copy-start | bytes 6148
  113.2 20.1 %copy-start.4 = (bf16[128,512]{1,0:T(8,128)(2,1)S(1)}, bf16[128,512]{1,0:T(8,128)(2,1)}, u32[]{:S(2)}) copy-start(bf16[128,512]{1,0:T(8,128)(2,1)} %param.15) | copy-start | bytes 393220
  113.3 32.6 %copy-start.6 = (bf16[1408,32]{0,1:T(8,128)(2,1)S(1)}, bf16[1408,32]{0,1:T(8,128)(2,1)}, u32[]{:S(2)}) copy-start(bf16[1408,32]{0,1:T(8,128)(2,1)} %param.27) | copy-start | bytes 270340
  113.3 32.6 %copy-start.7 = (bf16[32,1408]{1,0:T(8,128)(2,1)S(1)}, bf16[32,1408]{1,0:T(8,128)(2,1)}, u32[]{:S(2)}) copy-start(bf16[32,1408]{1,0:T(8,128)(2,1)} %param.26) | copy-start | bytes 270340
  113.3 32.6 %copy-start.8 = (bf16[32,1408]{1,0:T(8,128)(2,1)S(1)}, bf16[32,1408]{1,0:T(8,128)(2,1)}, u32[]{:S(2)}) copy-start(bf16[32,1408]{1,0:T(8,128)(2,1)} %param.25) | copy-start | bytes 270340
  114.6 7.7 %all-to-all-start = ((f32[4,1,128]{2,1,0:T(1,128)}), f32[4,1,128]{2,1,0:T(1,128)S(1)}, u32[]{:S(2)}, u32[]{:S(2)}) async-start(f32[4,1,128]{2,1,0:T(1,128)} %broadcast_in_dim.49), calls=%async_computation | async-start | bytes 4096 | tf_op jit(solution)/shard_map/all_to_all | solution.py:81
  134.0 7.3 %all-to-all-start.2 = ((f32[4,1,128]{2,1,0:T(1,128)}), f32[4,1,128]{2,1,0:T(1,128)S(1)}, u32[]{:S(2)}, u32[]{:S(2)}) async-start(f32[4,1,128]{2,1,0:T(1,128)} %broadcast_in_dim.50), calls=%async_computation.2 | async-start | bytes 4096 | tf_op jit(solution)/shard_map/all_to_all | solution.py:81
  142.4 10.4 %all-to-all-start.3 = ((bf16[4,128,512]{1,2,0:T(8,128)(2,1)}), bf16[4,128,512]{1,2,0:T(8,128)(2,1)S(1)}, u32[]{:S(2)}, u32[]{:S(2)}) async-start(bf16[4,128,512]{1,2,0:T(8,128)(2,1)} %broadcast_in_dim.51), calls=%async_computation.3 | async-start | bytes 1048576 | tf_op jit(solution)/shard_map/all_to_all | solution.py:81
  (25 other events, 131.6 us)
Sparse Core Ops, SparseCore 0:
  20.8 25.6 all-gather.8
  51.9 39.3 all-gather.10
